TPU v7x, 32 devices: a whole 2x2x4 slice. The times are simulated.
32 devices in a mesh: rep: 2 (over y), fs: 4 (over z), tp: 4 (over x, core).
Axes of the slice: x: 2, y: 2, z: 4, core: 2. Of those that a mesh axis runs over, the one named last changes fastest.
Arguments:
- activations: bfloat16 [8, 256, 2048], P(('rep', 'fs'), None, 'tp'), may hold values from -15 to 15
- norm_gain: float32 [2048], replicated, may hold values from 0.1 to 1.9
- w_value: bfloat16 [2048, 2048], P('fs', 'tp'), may hold values from -0.125 to 0.125
- w_gate_conv: bfloat16 [2048, 2048], P('fs', 'tp'), may hold values from -0.125 to 0.125
- conv_weight: float32 [31, 2048], P(None, 'tp'), may hold values from -3 to 3
- chan_gain: float32 [2048], P('tp'), may hold values from 0.1 to 1.9
- w_conv_out: bfloat16 [2048, 2048], P('tp', 'fs'), may hold values from -0.125 to 0.125
- mix_gain: float32 [2048], replicated, may hold values from 0.1 to 1.9
- w_gate: bfloat16 [2048, 3072], P('fs', 'tp'), may hold values from -0.125 to 0.125
- w_up: bfloat16 [2048, 3072], P('fs', 'tp'), may hold values from -0.125 to 0.125
- w_down: bfloat16 [3072, 2048], P('tp', 'fs'), may hold values from -0.109375 to 0.109375
- final_gain: float32 [2048], P('tp'), may hold values from 0.1 to 1.9
Outputs:
- result: bfloat16 [8, 256, 2048], P(('rep', 'fs'), None, 'tp')
All inputs are finite; a program needn't handle non-finite values.
Results may differ from a plain program's by a relative error of at most 0.013.
Values may be sent and summed in bfloat16 or wider, within the bound.
A program may use at most 64 MiB of HBM per device.

v0:
```python
import jax
import jax.numpy as jnp
from jax import lax
from jax.sharding import PartitionSpec as P

EPS = 1e-06


def body(
    activations,
    norm_gain,
    w_value,
    w_gate_conv,
    conv_weight,
    chan_gain,
    w_conv_out,
    mix_gain,
    w_gate,
    w_up,
    w_down,
    final_gain,
):
    batch, length, local_width = activations.shape
    width = local_width * lax.axis_size("tp")
    count = batch * length
    residual = activations.reshape(count, local_width).astype(jnp.float32)
    raw_in = lax.all_gather(
        activations.reshape(count, local_width), "tp", axis=1, tiled=True
    ).astype(jnp.float32)
    in_mean = jnp.mean(raw_in * raw_in, axis=1, keepdims=True)
    rows_in = (raw_in * lax.rsqrt(in_mean + EPS) * norm_gain).astype(jnp.bfloat16)
    chan_local = w_value.shape[1]
    pieces = (
        lax.all_gather(w_value, "fs", axis=0, tiled=True),
        lax.all_gather(w_gate_conv, "fs", axis=0, tiled=True),
    )
    columns = rows_in
    value = jnp.dot(columns, pieces[0], preferred_element_type=jnp.float32)
    gate_conv = jnp.dot(columns, pieces[1], preferred_element_type=jnp.float32)
    glu = (value * jax.nn.sigmoid(gate_conv)).reshape(batch, length, chan_local)
    taps = conv_weight.shape[0]
    padded = jnp.pad(glu, ((0, 0), (taps - 1, 0), (0, 0)))
    conv = lax.conv_general_dilated(
        padded,
        conv_weight[:, None, :],
        (1,),
        "VALID",
        dimension_numbers=("NWC", "WIO", "NWC"),
        feature_group_count=chan_local,
        precision=lax.Precision.HIGHEST,
    ).reshape(count, chan_local)
    chan_total = chan_local * lax.axis_size("tp")
    mean = lax.psum(jnp.sum(conv, axis=1), "tp") / chan_total
    centered = conv - mean[:, None]
    spread = lax.psum(jnp.sum(centered * centered, axis=1), "tp") / chan_total
    act = jax.nn.silu(centered * lax.rsqrt(spread + EPS)[:, None] * chan_gain).astype(jnp.bfloat16)
    conv_terms = jnp.dot(
        act,
        lax.all_gather(w_conv_out, "fs", axis=1, tiled=True),
        preferred_element_type=jnp.float32,
    )
    conv_out = lax.psum_scatter(
        conv_terms.astype(jnp.bfloat16), "tp", scatter_dimension=1, tiled=True
    ).astype(jnp.float32)
    first = (residual + conv_out).astype(jnp.bfloat16)
    first_f = first.astype(jnp.float32)
    raw_mid = lax.all_gather(first, "tp", axis=1, tiled=True).astype(jnp.float32)
    mid_mean = jnp.mean(raw_mid * raw_mid, axis=1, keepdims=True)
    rows_mid = (raw_mid * lax.rsqrt(mid_mean + EPS) * mix_gain).astype(jnp.bfloat16)
    hidden_local = w_gate.shape[1]
    zero_hidden = jnp.zeros((count, hidden_local), jnp.float32)
    pieces = (
        lax.all_gather(w_gate, "fs", axis=0, tiled=True),
        lax.all_gather(w_up, "fs", axis=0, tiled=True),
    )
    columns = lax.slice_in_dim(rows_mid, 0, pieces[0].shape[0], axis=1)
    gate = zero_hidden + jnp.dot(columns, pieces[0], preferred_element_type=jnp.float32)
    up = zero_hidden + jnp.dot(columns, pieces[1], preferred_element_type=jnp.float32)
    hidden = (jax.nn.silu(gate) * up).astype(jnp.bfloat16)
    ff_terms = jnp.dot(
        hidden, lax.all_gather(w_down, "fs", axis=1, tiled=True), preferred_element_type=jnp.float32
    )
    ff_out = lax.psum_scatter(
        ff_terms.astype(jnp.bfloat16), "tp", scatter_dimension=1, tiled=True
    ).astype(jnp.float32)
    second = first_f + ff_out
    out_total = lax.psum(jnp.sum(second * second, axis=1), "tp")
    result = (second * lax.rsqrt(out_total / width + EPS)[:, None] * final_gain).astype(
        jnp.bfloat16
    )
    return result.reshape(batch, length, local_width)


def solution(mesh):
    in_specs = (
        P(("rep", "fs"), None, "tp"),
        P(),
        P("fs", "tp"),
        P("fs", "tp"),
        P(None, "tp"),
        P("tp"),
        P("tp", "fs"),
        P(),
        P("fs", "tp"),
        P("fs", "tp"),
        P("tp", "fs"),
        P("tp"),
    )
    out_specs = P(("rep", "fs"), None, "tp")
    return jax.shard_map(body, mesh=mesh, in_specs=in_specs, out_specs=out_specs, check_vma=False)
```

profile of v0, /device:TPU:0, one launch (start us, length us, event | category | flops | bytes accessed | tf_op | source)
XLA Modules:
  0.0 451.0 jit_solution(17801474472369738869)
XLA Ops:
  6.5 0.7 all-gather.24.cloned.1.call-update
  7.3 0.0 all-gather.12.cloned.1.call-start
  7.3 0.7 all-gather.12.cloned.1.call-update
  8.0 0.0 all-gather.10.cloned.1.call-start
  8.1 0.7 all-gather.10.cloned.1.call-update
  8.7 0.0 all-gather.14.cloned.1.call-start
  8.8 0.5 all-gather.14.cloned.1.call-update
  9.3 0.0 reduce-scatter.3.cloned.1.call-start
  9.4 19.0 %all-gather.24.cloned.1.call-done = bf16[1,256,2048]{2,1,0:T(8,128)(2,1)} async-done(((bf16[1,256,512]{2,1,0:T(8,128)(2,1)}), bf16[1,256,2048]{2,1,0:T(8,128)(2,1)}) %all-gather.24.cloned.1.call-update) | async-done | bytes 1048592 | tf_op jit(solution)/shard_map/all_gather | solution.py:27
  28.4 1.5 fusion.3
  29.9 45.7 %all-gather.12.cloned.1.call-done = bf16[2048,512]{1,0:T(8,128)(2,1)} async-done(((bf16[512,512]{1,0:T(8,128)(2,1)}), bf16[2048,512]{1,0:T(8,128)(2,1)}) %all-gather.12.cloned.1.call-update) | async-done | bytes 2097168 | tf_op jit(solution)/shard_map/all_gather | solution.py:35
  75.6 2.8 fusion.10
  78.4 43.3 %all-gather.10.cloned.1.call-done = bf16[2048,512]{1,0:T(8,128)(2,1)} async-done(((bf16[512,512]{1,0:T(8,128)(2,1)}), bf16[2048,512]{1,0:T(8,128)(2,1)}) %all-gather.10.cloned.1.call-update) | async-done | bytes 2097168 | tf_op jit(solution)/shard_map/all_gather | solution.py:34
  121.7 2.3 fusion.7
  124.0 0.1 pad.2
  124.1 0.7 reshape.42
  124.8 0.2 copy.18
  125.0 0.1 slice.2
  125.1 1.2 convolution_select_fusion
  126.3 0.3 copy.20
  126.7 0.1 reshape.46
  126.8 0.1 slice_reduce_fusion
  126.9 6.4 %psum.21 = f32[256]{0:T(256)S(1)} all-reduce(f32[256]{0:T(256)S(1)} %slice_reduce_fusion), channel_id=1, replica_groups=mesh['rep'=2,'fs'=4,'tp'=4] {'tp'}, use_global_device_ids=true, to_apply=%region_2.3 | all-reduce | flops 256 | bytes 2048 | tf_op jit(solution)/shard_map/psum | solution.py:53
  133.3 0.2 multiply_reduce_fusion.1
  133.5 6.3 %psum.22 = f32[256]{0:T(256)S(1)} all-reduce(f32[256]{0:T(256)S(1)} %multiply_reduce_fusion.1), channel_id=1, replica_groups=mesh['rep'=2,'fs'=4,'tp'=4] {'tp'}, use_global_device_ids=true, to_apply=%region_4.5 | all-reduce | flops 256 | bytes 2048 | tf_op jit(solution)/shard_map/psum | solution.py:55
  139.8 27.8 %all-gather.14.cloned.1.call-done = bf16[512,2048]{1,0:T(8,128)(2,1)} async-done(((bf16[512,512]{1,0:T(8,128)(2,1)}), bf16[512,2048]{1,0:T(8,128)(2,1)}) %all-gather.14.cloned.1.call-update) | async-done | bytes 2097168 | tf_op jit(solution)/shard_map/all_gather | solution.py:59
  167.6 3.4 convolution_convert_fusion
  171.1 0.0 all-gather.16.cloned.1.call-start
  171.1 23.7 %reduce-scatter.3.cloned.1.call-done = bf16[256,512]{1,0:T(8,128)(2,1)} async-done(((bf16[256,2048]{1,0:T(8,128)(2,1)}), bf16[256,512]{1,0:T(8,128)(2,1)}) %reduce-scatter.3.cloned.1.call-update) | async-done | bytes 262160 | tf_op jit(solution)/shard_map/reduce_scatter | solution.py:62
  194.8 1.7 fusion.17
  196.6 0.0 all-gather.18.cloned.1.call-start
  196.6 0.7 all-gather.18.cloned.1.call-update
  197.3 0.0 all-gather.20.cloned.1.call-start
  197.4 0.7 all-gather.20.cloned.1.call-update
  198.1 0.0 all-gather.22.cloned.1.call-start
  198.1 0.7 all-gather.22.cloned.1.call-update
  198.8 0.0 reduce-scatter.5.cloned.1.call-start
  198.8 14.6 %all-gather.16.cloned.1.call-done = bf16[256,2048]{1,0:T(8,128)(2,1)} async-done(((bf16[256,512]{1,0:T(8,128)(2,1)}), bf16[256,2048]{1,0:T(8,128)(2,1)}) %all-gather.16.cloned.1.call-update) | async-done | bytes 1048592 | tf_op jit(solution)/shard_map/all_gather | solution.py:67
  213.4 1.5 fusion
  215.0 63.5 %all-gather.18.cloned.1.call-done = bf16[2048,768]{1,0:T(8,128)(2,1)} async-done(((bf16[512,768]{1,0:T(8,128)(2,1)}), bf16[2048,768]{1,0:T(8,128)(2,1)}) %all-gather.18.cloned.1.call-update) | async-done | bytes 3145744 | tf_op jit(solution)/shard_map/all_gather | solution.py:73
  278.5 3.2 fusion.23
  281.8 60.4 %all-gather.20.cloned.1.call-done = bf16[2048,768]{1,0:T(8,128)(2,1)} async-done(((bf16[512,768]{1,0:T(8,128)(2,1)}), bf16[2048,768]{1,0:T(8,128)(2,1)}) %all-gather.20.cloned.1.call-update) | async-done | bytes 3145744 | tf_op jit(solution)/shard_map/all_gather | solution.py:74
  342.2 63.7 %all-gather.22.cloned.1.call-done = bf16[768,2048]{1,0:T(8,128)(2,1)} async-done(((bf16[768,512]{1,0:T(8,128)(2,1)}), bf16[768,2048]{1,0:T(8,128)(2,1)}) %all-gather.22.cloned.1.call-update) | async-done | bytes 3145744 | tf_op jit(solution)/shard_map/all_gather | solution.py:81
  405.9 6.0 %convolution_convert_fusion.1 = bf16[256,2048]{1,0:T(8,128)(2,1)} fusion(bf16[768,2048]{1,0:T(8,128)(2,1)} %all-gather.22.cloned.1.call-done, bf16[2048,768]{1,0:T(8,128)(2,1)} %all-gather.20.cloned.1.call-done, f32[256,768]{1,0:T(8,128)S(1)} %fusion.23, bf16[256,2048]{1,0:T(8,128)(2,1)S(1)} %copy-done.3, f32[2048]{0:T(1024)S(1)} %copy-done.7, ...), kind=kOutput, calls=%fused_computation.5 | convolution fusion | flops 1614413824 | bytes 9184256 | tf_op jit(solution)/shard_map/dot_general | solution.py:80
  411.9 23.6 %reduce-scatter.5.cloned.1.call-done = bf16[256,512]{1,0:T(8,128)(2,1)} async-done(((bf16[256,2048]{1,0:T(8,128)(2,1)}), bf16[256,512]{1,0:T(8,128)(2,1)}) %reduce-scatter.5.cloned.1.call-update) | async-done | bytes 262160 | tf_op jit(solution)/shard_map/reduce_scatter | solution.py:83
  435.5 1.1 multiply_reduce_fusion
  436.6 5.8 %psum.23 = f32[256]{0:T(256)S(1)} all-reduce(f32[256]{0:T(256)S(1)} %multiply_reduce_fusion), channel_id=1, replica_groups=mesh['rep'=2,'fs'=4,'tp'=4] {'tp'}, use_global_device_ids=true, to_apply=%region_9.10 | all-reduce | flops 256 | bytes 2048 | tf_op jit(solution)/shard_map/psum | solution.py:87
  442.4 1.8 fusion.25
  (29 shorter events, 0.1 us)
Async XLA Ops:
  6.5 118.5 %copy-start = (f32[31,512]{1,0:T(8,128)S(1)}, f32[31,512]{1,0:T(8,128)}, u32[]{:S(2)}) copy-start(f32[31,512]{1,0:T(8,128)} %param.16) | copy-start | bytes 190468
  6.5 69.1 %copy-start.6 = (f32[2048]{0:T(1024)S(1)}, f32[2048]{0:T(1024)}, u32[]{:S(2)}) copy-start(f32[2048]{0:T(1024)} %param.13) | copy-start | bytes 24580
  6.5 21.8 %all-gather.24.cloned.1.call-start = ((), (), s32[]{:S(2)}) async-start(), calls=%async_computation.11 | async-start | bytes 1310720 | tf_op jit(solution)/shard_map/all_gather | solution.py:27
  7.3 68.3 %all-gather.12.cloned.1.call-start = ((), (), s32[]{:S(2)}) async-start(), calls=%async_computation.3 | async-start | bytes 2621440 | tf_op jit(solution)/shard_map/all_gather | solution.py:35
  8.0 113.7 %all-gather.10.cloned.1.call-start = ((), (), s32[]{:S(2)}) async-start(), calls=%async_computation.2 | async-start | bytes 2621440 | tf_op jit(solution)/shard_map/all_gather | solution.py:34
  8.7 158.9 %all-gather.14.cloned.1.call-start = ((), (), s32[]{:S(2)}) async-start(), calls=%async_computation.4 | async-start | bytes 2621440 | tf_op jit(solution)/shard_map/all_gather | solution.py:59
  9.3 185.5 %reduce-scatter.3.cloned.1.call-start = ((), (), s32[]{:S(2)}) async-start(), calls=%async_computation.5 | async-start | bytes 1310720 | tf_op jit(solution)/shard_map/reduce_scatter | solution.py:62
  29.9 91.8 %copy-start.4 = (bf16[1,256,2048]{2,1,0:T(8,128)(2,1)S(1)}, bf16[1,256,2048]{2,1,0:T(8,128)(2,1)}, u32[]{:S(2)}) copy-start(bf16[1,256,2048]{2,1,0:T(8,128)(2,1)} %all-gather.24.cloned.1.call-done) | copy-start | bytes 3145732
  124.0 1.0 copy-start.9
  126.3 41.3 %copy-start.8 = (f32[512]{0:T(512)S(1)}, f32[512]{0:T(512)}, u32[]{:S(2)}) copy-start(f32[512]{0:T(512)} %param.17) | copy-start | bytes 6148
  139.8 55.1 %copy-start.2 = (bf16[1,256,512]{2,1,0:T(8,128)(2,1)S(1)}, bf16[1,256,512]{2,1,0:T(8,128)(2,1)}, u32[]{:S(2)}) copy-start(bf16[1,256,512]{2,1,0:T(8,128)(2,1)} %param.12) | copy-start | bytes 786436
  171.1 107.4 %copy-start.7 = (f32[2048]{0:T(1024)S(1)}, f32[2048]{0:T(1024)}, u32[]{:S(2)}) copy-start(f32[2048]{0:T(1024)} %param.19) | copy-start | bytes 24580
  171.1 42.4 %all-gather.16.cloned.1.call-start = ((), (), s32[]{:S(2)}) async-start(), calls=%async_computation.6 | async-start | bytes 1310720 | tf_op jit(solution)/shard_map/all_gather | solution.py:67
  196.6 81.9 %all-gather.18.cloned.1.call-start = ((), (), s32[]{:S(2)}) async-start(), calls=%async_computation.7 | async-start | bytes 3932160 | tf_op jit(solution)/shard_map/all_gather | solution.py:73
  197.3 144.8 %all-gather.20.cloned.1.call-start = ((), (), s32[]{:S(2)}) async-start(), calls=%async_computation.8 | async-start | bytes 3932160 | tf_op jit(solution)/shard_map/all_gather | solution.py:74
  198.1 207.8 %all-gather.22.cloned.1.call-start = ((), (), s32[]{:S(2)}) async-start(), calls=%async_computation.9 | async-start | bytes 3932160 | tf_op jit(solution)/shard_map/all_gather | solution.py:81
  198.8 236.7 %reduce-scatter.5.cloned.1.call-start = ((), (), s32[]{:S(2)}) async-start(), calls=%async_computation.10 | async-start | bytes 1310720 | tf_op jit(solution)/shard_map/reduce_scatter | solution.py:83
  214.9 190.9 %copy-start.3 = (bf16[256,2048]{1,0:T(8,128)(2,1)S(1)}, bf16[256,2048]{1,0:T(8,128)(2,1)}, u32[]{:S(2)}) copy-start(bf16[256,2048]{1,0:T(8,128)(2,1)} %all-gather.16.cloned.1.call-done) | copy-start | bytes 3145732
  281.7 153.8 %copy-start.1 = (bf16[256,512]{1,0:T(8,128)(2,1)S(1)}, bf16[256,512]{1,0:T(8,128)(2,1)}, u32[]{:S(2)}) copy-start(bf16[256,512]{1,0:T(8,128)(2,1)} %fusion.17) | copy-start | bytes 786436
  281.7 160.6 %copy-start.5 = (f32[512]{0:T(512)S(1)}, f32[512]{0:T(512)}, u32[]{:S(2)}) copy-start(f32[512]{0:T(512)} %param.23) | copy-start | bytes 6148
Sparse Core Ops, SparseCore 0:
  8.9 19.4 all-gather.23
  29.9 45.6 all-gather.11
  77.2 44.4 all-gather.9
  123.1 44.4 all-gather.13
  171.2 23.6 reduce-scatter.2
  196.7 16.6 all-gather.15
  215.0 63.4 all-gather.17
  280.0 62.0 all-gather.19
  343.7 62.0 all-gather.21
  412.0 23.4 reduce-scatter.4
where the time goes:
time: 451 us
  waiting for transfers between devices  390 us (86%)
  matrix products  19 us (4%)
  blocking collectives  18.4 us (4%)
  between operations  13.7 us (3%)
  other arithmetic  7.97 us (2%)
    all_gather x1, waiting for transfers between devices, body(): lax.all_gather(w_down, 'fs', axis=1, tiled=True)  63.7 us
    all_gather x1, waiting for transfers between devices, body(): lax.all_gather(w_gate, 'fs', axis=0, tiled=True)  63.5 us
    all_gather x1, waiting for transfers between devices, body(): lax.all_gather(w_up, 'fs', axis=0, tiled=True)  60.4 us
    all_gather x1, waiting for transfers between devices, body(): lax.all_gather(w_gate_conv, 'fs', axis=0, tiled=True)  45.7 us
    all_gather x1, waiting for transfers between devices, body(): lax.all_gather(w_value, 'fs', axis=0, tiled=True)  43.3 us
    all_gather x1, waiting for transfers between devices, body(): lax.all_gather(w_conv_out, 'fs', axis=1, tiled=True)  27.8 us
    reduce_scatter x1, waiting for transfers between devices, body(): lax.psum_scatter(conv_terms.astype(jnp.bfloat16), 'tp', scatter_dimension...  23.7 us
    reduce_scatter x1, waiting for transfers between devices, body(): lax.psum_scatter(ff_terms.astype(jnp.bfloat16), 'tp', scatter_dimension=1...  23.6 us
  transfers between devices with their start and end apart: 10, of which 10 were waited for; matrix products, arithmetic and copies ran while one was open for 3% of the time, Pallas kernels for 0%

commit v1 on v0

v1 whole, which is shorter than its diff:
```python
import functools

import jax
import jax.numpy as jnp
from jax import lax
from jax.experimental import pallas as pl
from jax.experimental.pallas import tpu as pltpu
from jax.sharding import PartitionSpec as P

EPS = 1e-06
MESH = pl.DeviceIdType.MESH
F32 = jnp.float32
BF16 = jnp.bfloat16


def remote(src, dst, send, recv, target):
    return pltpu.make_async_remote_copy(
        src_ref=src, dst_ref=dst, send_sem=send, recv_sem=recv, device_id=target, device_id_type=MESH
    )


def chunk_of(extent, want):
    return want if extent % want == 0 else extent


def kernel(
    R, F, T, split, length,
    x_ref, ng_ref, cw_ref, cg_ref, mg_ref, fg_ref,
    wv_ref, wg_ref, wo_ref, wga_ref, wup_ref, wd_ref,
    out_ref,
    bv, bg, bo, bga, bup, bd,
    xg, rows, glu, conv, act, part1, part2, got1, got2, firsts, hid, st1, st2, sg1, sg2,
    own_sem, zs, zr, ys, yr, ts, tr,
):
    f = lax.axis_index("fs")
    me = lax.axis_index("tp")
    rep = lax.axis_index("rep")
    count, dt = x_ref.shape
    width = dt * T
    local = [wv_ref, wg_ref, wo_ref, wga_ref, wup_ref, wd_ref]
    bufs = [bv, bg, bo, bga, bup, bd]

    barrier = pltpu.get_barrier_semaphore()
    greeted = 0
    for target in (lax.rem(f + 1, F), lax.rem(f + F - 1, F)):
        pl.semaphore_signal(barrier, inc=1, device_id={"fs": target}, device_id_type=MESH)
        greeted += 1
    if split == 2:
        pl.semaphore_signal(barrier, inc=1, device_id={"rep": 1 - rep}, device_id_type=MESH)
        greeted += 1
    for d in range(1, T):
        pl.semaphore_signal(barrier, inc=1, device_id={"tp": lax.rem(me + d, T)}, device_id_type=MESH)
        greeted += 1
    own = [
        pltpu.make_async_copy(local[w], bufs[w].at[f], own_sem.at[w]) for w in range(6)
    ]
    for copy in own:
        copy.start()
    pl.semaphore_wait(barrier, greeted)

    def half(w):
        n = local[w].shape[0] // split
        return pl.ds(pl.multiple_of((rep if split == 2 else 0) * n, n), n)

    def other(w):
        n = local[w].shape[0] // split
        return pl.ds(pl.multiple_of((1 - rep) * n, n), n)

    def hop(w, side, s):
        shard = f - s if side == 0 else f + s
        target = f + 1 if side == 0 else f - 1
        src = local[w].at[half(w)] if s == 0 else bufs[w].at[shard, half(w)]
        return remote(src, bufs[w].at[shard, half(w)], zs.at[side, w, s], zr.at[side, w, s + 1], {"fs": target})

    def arrival(w, side, s):
        shard = f - s if side == 0 else f + s
        ref = bufs[w].at[shard, half(w)]
        return remote(ref, ref, zs.at[side, w, s], zr.at[side, w, s], {"fs": f})

    def across(w, side, s):
        shard = f - s if side == 0 else f + s
        ref = bufs[w].at[shard, half(w)]
        return remote(ref, ref, ys.at[side, w, s], yr.at[side, w, s], {"rep": 1 - rep})

    def across_in(w, side, s):
        shard = f - s if side == 0 else f + s
        ref = bufs[w].at[shard, other(w)]
        return remote(ref, ref, ys.at[side, w, s], yr.at[side, w, s], {"rep": 1 - rep})

    def has(side, s):
        return f >= s if side == 0 else f + s <= F - 1

    def sends(side, s):
        ahead = f < F - 1 if side == 0 else f > 0
        return jnp.logical_and(has(side, s), ahead)

    def launch(w):
        for side in (0, 1):
            @pl.when(sends(side, 0))
            def _():
                hop(w, side, 0).start()

    def relay(group):
        for s in range(1, F):
            for w in group:
                for side in (0, 1):
                    @pl.when(has(side, s))
                    def _():
                        arrival(w, side, s).wait_recv()
                        if s < F - 1:
                            @pl.when(sends(side, s))
                            def _():
                                hop(w, side, s).start()
                        if split == 2:
                            across(w, side, s).start()

    def settle(group):
        for w in group:
            own[w].wait()
        if split == 2:
            for s in range(1, F):
                for w in group:
                    for side in (0, 1):
                        @pl.when(has(side, s))
                        def _():
                            across_in(w, side, s).wait_recv()

    def tp_send(k, src, dst_at, d):
        return remote(src, dst_at, ts.at[k, d], tr.at[k, d], {"tp": lax.rem(me + d, T)})

    for w in (0, 1):
        launch(w)
    for d in range(1, T):
        tp_send(0, x_ref, xg.at[me], d).start()
    launch(2)
    xg[me] = x_ref[...]
    for d in range(1, T):
        peer = lax.rem(me + T - d, T)
        tp_send(0, x_ref, xg.at[peer], d).wait_recv()

    block = chunk_of(count, 16)

    def norm_rows(src, gain):
        def step(i, _):
            r = pl.ds(pl.multiple_of(i * block, block), block)
            vals = [src[t, r, :].astype(F32) for t in range(T)]
            ss = sum(jnp.sum(v * v, axis=1, keepdims=True) for v in vals)
            scale = lax.rsqrt(ss / width + EPS)
            for t in range(T):
                rows[r, t * dt:(t + 1) * dt] = (
                    vals[t] * scale * gain[t:t + 1, :]
                ).astype(BF16)
            return 0
        lax.fori_loop(0, count // block, step, 0)

    norm_rows(xg, ng_ref)
    relay((0, 1))
    launch(3)
    launch(4)
    settle((0, 1))

    chan = bv.shape[2]
    batch = count // length
    taps = cw_ref.shape[0]
    pad = 8 * ((taps - 1 + 7) // 8)
    lead = pad - (taps - 1)

    def columns(buf, c, n):
        block_w = buf[:, :, pl.ds(pl.multiple_of(c * n, n), n)]
        return block_w.reshape(block_w.shape[0] * block_w.shape[1], n)

    nc = chunk_of(chan, 256)

    def glu_step(c, _):
        value = jnp.dot(rows[...], columns(bv, c, nc), preferred_element_type=F32)
        gate = jnp.dot(rows[...], columns(bg, c, nc), preferred_element_type=F32)
        res = value * jax.nn.sigmoid(gate)
        for b in range(batch):
            glu[b, pl.ds(pad, length), pl.ds(pl.multiple_of(c * nc, nc), nc)] = (
                res[b * length:(b + 1) * length]
            )
        return 0

    for b in range(batch):
        glu[b, 0:pad, :] = jnp.zeros((pad, chan), F32)
        glu[b, pad + length:, :] = jnp.zeros((8, chan), F32)
    lax.fori_loop(0, chan // nc, glu_step, 0)

    lanes = chunk_of(chan, 128)
    span = chunk_of(length, 64)
    strips = chan // lanes

    def conv_step(i, _):
        q = lax.rem(i, strips)
        p = i // strips
        cols = pl.ds(pl.multiple_of(q * lanes, lanes), lanes)
        weights = cw_ref[:, cols]
        for b in range(batch):
            total = jnp.zeros((span, lanes), F32)
            for shift in range(8):
                acc = None
                for tap in range(taps):
                    if (lead + tap) % 8 != shift:
                        continue
                    base = lead + tap - shift
                    term = weights[tap:tap + 1, :] * glu[
                        b, pl.ds(pl.multiple_of(p * span + base, 8), span + 8), cols
                    ]
                    acc = term if acc is None else acc + term
                if acc is not None:
                    total = total + acc[shift:shift + span]
            conv[pl.ds(pl.multiple_of(b * length + p * span, span), span), cols] = total
        return 0

    lax.fori_loop(0, strips * (length // span), conv_step, 0)

    lane = lax.broadcasted_iota(jnp.int32, (count, 128), 1)

    def across_lanes(a, b):
        table = jnp.where(lane == 0, a, jnp.where(lane == 1, b, 0.0))
        return jnp.transpose(table)[0:8, :]

    def down_rows(top):
        full = jnp.concatenate([top, jnp.zeros((120, count), F32)], axis=0)
        return jnp.transpose(full)

    values = conv[...]
    local_sum = jnp.sum(values, axis=1, keepdims=True)
    dev = values - local_sum / chan
    st1[...] = across_lanes(local_sum, jnp.sum(dev * dev, axis=1, keepdims=True))
    sg1[me] = st1[...]
    for d in range(1, T):
        tp_send(1, st1, sg1.at[me], d).start()
    relay((2,))
    launch(5)
    for d in range(1, T):
        peer = lax.rem(me + T - d, T)
        tp_send(1, st1, sg1.at[peer], d).wait_recv()
    sums = [sg1[t] for t in range(T)]
    mean = sum(s[0:1, :] for s in sums) / (chan * T)
    spread = sum(
        s[1:2, :] + chan * (s[0:1, :] / chan - mean) * (s[0:1, :] / chan - mean) for s in sums
    ) / (chan * T)
    inv = lax.rsqrt(spread + EPS)
    line = lax.broadcasted_iota(jnp.int32, (8, count), 0)
    table = down_rows(jnp.where(line == 0, mean, jnp.where(line == 1, inv, 0.0)))
    normed = (conv[...] - table[:, 0:1]) * table[:, 1:2] * cg_ref[...]
    act[...] = (normed * jax.nn.sigmoid(normed)).astype(BF16)

    settle((2,))

    def project(src, buf, part):
        dsh = buf.shape[2]
        for j in range(F):
            t, off = (j * dsh) // dt, (j * dsh) % dt
            prod = jnp.dot(src[...], buf[j], preferred_element_type=F32)
            part[t, :, off:off + dsh] = prod.astype(BF16)

    def scatter(k, part, got):
        for d in range(1, T):
            tp_send(k, part.at[lax.rem(me + d, T)], got.at[d - 1], d).start()

    def gathered(k, part, got):
        total = part[me].astype(F32)
        for d in range(1, T):
            tp_send(k, part.at[me], got.at[d - 1], d).wait_recv()
            total = total + got[d - 1].astype(F32)
        return total

    project(act, bo, part1)
    scatter(2, part1, got1)
    first = (x_ref[...].astype(F32) + gathered(2, part1, got1)).astype(BF16)
    firsts[me] = first
    for d in range(1, T):
        tp_send(3, firsts.at[me], firsts.at[me], d).start()
    relay((3, 4))
    for d in range(1, T):
        peer = lax.rem(me + T - d, T)
        tp_send(3, firsts.at[peer], firsts.at[peer], d).wait_recv()
    norm_rows(firsts, mg_ref)
    settle((3, 4))

    ff = bga.shape[2]
    nf = chunk_of(ff, 256)

    def ff_step(c, _):
        gate = jnp.dot(rows[...], columns(bga, c, nf), preferred_element_type=F32)
        up = jnp.dot(rows[...], columns(bup, c, nf), preferred_element_type=F32)
        hid[:, pl.ds(pl.multiple_of(c * nf, nf), nf)] = (
            gate * jax.nn.sigmoid(gate) * up
        ).astype(BF16)
        return 0

    lax.fori_loop(0, ff // nf, ff_step, 0)
    relay((5,))
    settle((5,))
    project(hid, bd, part2)
    scatter(4, part2, got2)
    second = firsts[me].astype(F32) + gathered(4, part2, got2)
    total = jnp.sum(second * second, axis=1, keepdims=True)
    conv[:, 0:dt] = second
    st2[...] = across_lanes(total, total)
    sg2[me] = st2[...]
    for d in range(1, T):
        tp_send(5, st2, sg2.at[me], d).start()
    for d in range(1, T):
        peer = lax.rem(me + T - d, T)
        tp_send(5, st2, sg2.at[peer], d).wait_recv()
    full = sum(sg2[t] for t in range(T))
    table = down_rows(full)
    scale = lax.rsqrt(table[:, 0:1] / width + EPS)
    out_ref[...] = (conv[:, 0:dt] * scale * fg_ref[...]).astype(BF16)

    for w in range(6):
        for side in (0, 1):
            for s in range(F):
                if s < F - 1:
                    @pl.when(sends(side, s))
                    def _():
                        hop(w, side, s).wait_send()
                if s >= 1 and split == 2:
                    @pl.when(has(side, s))
                    def _():
                        across(w, side, s).wait_send()
    for d in range(1, T):
        peer = lax.rem(me + d, T)
        tp_send(0, x_ref, xg.at[me], d).wait_send()
        tp_send(1, st1, sg1.at[me], d).wait_send()
        tp_send(2, part1.at[peer], got1.at[d - 1], d).wait_send()
        tp_send(3, firsts.at[me], firsts.at[me], d).wait_send()
        tp_send(4, part2.at[peer], got2.at[d - 1], d).wait_send()
        tp_send(5, st2, sg2.at[me], d).wait_send()


def body(
    activations, norm_gain, w_value, w_gate_conv, conv_weight, chan_gain,
    w_conv_out, mix_gain, w_gate, w_up, w_down, final_gain,
):
    batch, length, dt = activations.shape
    count = batch * length
    R, F, T = lax.axis_size("rep"), lax.axis_size("fs"), lax.axis_size("tp")
    weights = (w_value, w_gate_conv, w_conv_out, w_gate, w_up, w_down)
    split = 2 if R == 2 and all(w.shape[0] % 32 == 0 for w in weights) else 1
    width = dt * T
    chan, ff = w_value.shape[1], w_gate.shape[1]
    taps = conv_weight.shape[0]
    pad = 8 * ((taps - 1 + 7) // 8)
    vmem, hbm = pl.BlockSpec(memory_space=pltpu.VMEM), pl.BlockSpec(memory_space=pl.ANY)
    ysh = (2, 6, F) if split == 2 else (1,)
    dma = pltpu.SemaphoreType.DMA
    out = pl.pallas_call(
        functools.partial(kernel, R, F, T, split, length),
        out_shape=jax.ShapeDtypeStruct((count, dt), BF16),
        in_specs=[vmem] * 6 + [hbm] * 6,
        out_specs=vmem,
        scratch_shapes=[pltpu.VMEM((F,) + w.shape, BF16) for w in weights] + [
            pltpu.VMEM((T, count, dt), BF16),
            pltpu.VMEM((count, width), BF16),
            pltpu.VMEM((batch, pad + length + 8, chan), F32),
            pltpu.VMEM((count, max(chan, dt)), F32),
            pltpu.VMEM((count, chan), BF16),
            pltpu.VMEM((T, count, dt), BF16),
            pltpu.VMEM((T, count, dt), BF16),
            pltpu.VMEM((T - 1, count, dt), BF16),
            pltpu.VMEM((T - 1, count, dt), BF16),
            pltpu.VMEM((T, count, dt), BF16),
            pltpu.VMEM((count, ff), BF16),
            pltpu.VMEM((8, count), F32),
            pltpu.VMEM((8, count), F32),
            pltpu.VMEM((T, 8, count), F32),
            pltpu.VMEM((T, 8, count), F32),
            dma((6,)),
            dma((2, 6, F)),
            dma((2, 6, F)),
            dma(ysh),
            dma(ysh),
            dma((6, T)),
            dma((6, T)),
        ],
        compiler_params=pltpu.CompilerParams(
            collective_id=0, has_side_effects=True, vmem_limit_bytes=60 * 1024 * 1024
        ),
        name="block",
    )(
        activations.reshape(count, dt),
        norm_gain.reshape(T, dt),
        conv_weight,
        chan_gain.reshape(1, chan),
        mix_gain.reshape(T, dt),
        final_gain.reshape(1, dt),
        *weights,
    )
    return out.reshape(batch, length, dt)


def solution(mesh):
    in_specs = (
        P(("rep", "fs"), None, "tp"),
        P(),
        P("fs", "tp"),
        P("fs", "tp"),
        P(None, "tp"),
        P("tp"),
        P("tp", "fs"),
        P(),
        P("fs", "tp"),
        P("fs", "tp"),
        P("tp", "fs"),
        P("tp"),
    )
    out_specs = P(("rep", "fs"), None, "tp")
    return jax.shard_map(body, mesh=mesh, in_specs=in_specs, out_specs=out_specs, check_vma=False)
```

time: 451 us -> 193 us (0.43)
  waiting for transfers between devices: 390 us -> 0 us
  Pallas kernels: 0 us -> 190 us
  matrix products: 19 us -> 0 us
  blocking collectives: 18.4 us -> 0 us
  between operations: 13.7 us -> 0.01 us
  other arithmetic: 7.97 us -> 0 us
    all_gather x8 -> x0, waiting for transfers between devices: 338 us -> none  [the longest x1 63.7 us: body(): lax.all_gather(w_down, 'fs', axis=1, tiled=True)]
    pallas_call x0 -> x1, Pallas kernels: none -> 190 us  [body(): pl.pallas_call(functools.partial(kernel, R, F, T, split, length), out_sha...]
    reduce_scatter x2 -> x0, waiting for transfers between devices: 47.3 us -> none  [the longest x1 23.7 us: body(): lax.psum_scatter(conv_terms.astype(jnp.bfloat16), 'tp', scatter_dimension...]
    psum x3 -> x0, blocking collectives: 18.4 us -> none  [the longest x1 6.41 us: body(): mean = lax.psum(jnp.sum(conv, axis=1), 'tp') / chan_total]
    dot_general x5 -> x0, matrix products: 17.8 us -> none  [the longest x1 6.02 us: body(): jnp.dot(hidden, lax.all_gather(w_down, 'fs', axis=1, tiled=True), preferr...]
    unnamed x10 -> x0, waiting for transfers between devices: 4.73 us -> none
  transfers between devices with their start and end apart: 10 -> 0, of which waited for: 10 -> 0; matrix products, arithmetic and copies ran while one was open for 3% -> 0% of each run, Pallas kernels for 0% -> 0%
where the time goes in v1:
time: 193 us
  Pallas kernels  190 us (98%)
  local copies, waits for them, and re-layouts  3.59 us (2%)
    pallas_call x1, Pallas kernels, body(): pl.pallas_call(functools.partial(kernel, R, F, T, split, length), out_sha...  190 us

profile of v1, /device:TPU:0, one launch (start us, length us, event | category | flops | bytes accessed | tf_op | source)
XLA Modules:
  0.0 193.2 jit_solution(2648439397852424473)
XLA Ops:
  0.0 0.0 copy-start
  0.0 1.3 reshape.19.ng_ref
  1.3 0.0 copy-done
  1.3 0.6 reshape.21.mg_ref
  1.9 189.6 %block.1 = bf16[256,512]{1,0:T(8,128)(2,1)} custom-call(bf16[256,512]{1,0:T(8,128)(2,1)} %bitcast.5, f32[4,512]{1,0:T(4,128)} %reshape.19.ng_ref, f32[31,512]{1,0:T(8,128)} %cw_ref.1, f32[1,512]{1,0:T(1,128)} %bitcast.6, f32[4,512]{1,0:T(4,128)} %reshape.21.mg_ref, f32[1,512]{1,0:T(1,128)} %bitcast.7, bf16[512,512]{1,0:T(8,128)(2,1)} %wv_ref.1, ...), custom_call_target="tpu_custom_call" | custom-call | tf_op jit(solution)/shard_map/block/pallas_call | solution.py:351
  191.5 1.7 copy.14
Async XLA Ops:
  0.0 1.3 copy-start

commit v2 on v1

--- a/solution.py
+++ b/solution.py
@@ -100,8 +100,8 @@
             def _():
                 hop(w, side, 0).start()
 
-    def relay(group):
-        for s in range(1, F):
+    def relay(group, stages=range(1, F)):
+        for s in stages:
             for w in group:
                 for side in (0, 1):
                     @pl.when(has(side, s))
@@ -154,9 +154,9 @@
         lax.fori_loop(0, count // block, step, 0)
 
     norm_rows(xg, ng_ref)
-    relay((0, 1))
-    launch(3)
-    launch(4)
+    relay((0, 1, 2))
+    for w in (3, 4, 5):
+        launch(w)
     settle((0, 1))
 
     chan = bv.shape[2]
@@ -185,6 +185,7 @@
         glu[b, 0:pad, :] = jnp.zeros((pad, chan), F32)
         glu[b, pad + length:, :] = jnp.zeros((8, chan), F32)
     lax.fori_loop(0, chan // nc, glu_step, 0)
+    relay((3,), (1,))
 
     lanes = chunk_of(chan, 128)
     span = chunk_of(length, 64)
@@ -231,8 +232,7 @@
     sg1[me] = st1[...]
     for d in range(1, T):
         tp_send(1, st1, sg1.at[me], d).start()
-    relay((2,))
-    launch(5)
+    relay((4,), (1,))
     for d in range(1, T):
         peer = lax.rem(me + T - d, T)
         tp_send(1, st1, sg1.at[peer], d).wait_recv()
@@ -267,17 +267,27 @@
             total = total + got[d - 1].astype(F32)
         return total
 
+    def piece(t):
+        return remote(part2.at[t], got2.at[me], ts.at[4, t], tr.at[4, me], {"tp": t})
+
+    def piece_in(t):
+        return remote(part2.at[t], got2.at[t], ts.at[4, t], tr.at[4, t], {"tp": t})
+
     project(act, bo, part1)
     scatter(2, part1, got1)
+    relay((5,), (1,))
     first = (x_ref[...].astype(F32) + gathered(2, part1, got1)).astype(BF16)
     firsts[me] = first
     for d in range(1, T):
         tp_send(3, firsts.at[me], firsts.at[me], d).start()
-    relay((3, 4))
+    relay((3,), (2,))
     for d in range(1, T):
         peer = lax.rem(me + T - d, T)
         tp_send(3, firsts.at[peer], firsts.at[peer], d).wait_recv()
+    relay((4,), (2,))
     norm_rows(firsts, mg_ref)
+    relay((5,), (2,))
+    relay((3, 4), range(3, F))
     settle((3, 4))
 
     ff = bga.shape[2]
@@ -292,11 +302,37 @@
         return 0
 
     lax.fori_loop(0, ff // nf, ff_step, 0)
-    relay((5,))
-    settle((5,))
-    project(hid, bd, part2)
-    scatter(4, part2, got2)
-    second = firsts[me].astype(F32) + gathered(4, part2, got2)
+    if F == T and bd.shape[2] == dt:
+        def down(shard):
+            prod = jnp.dot(hid[...], bd[shard], preferred_element_type=F32)
+            part2[shard] = prod.astype(BF16)
+
+            @pl.when(shard != me)
+            def _():
+                piece(shard).start()
+
+        own[5].wait()
+        down(f)
+        for s in range(1, F):
+            if s >= 3:
+                relay((5,), (s,))
+            for side in (0, 1):
+                @pl.when(has(side, s))
+                def _():
+                    if split == 2:
+                        across_in(5, side, s).wait_recv()
+                    down(f - s if side == 0 else f + s)
+    else:
+        relay((5,), range(3, F))
+        settle((5,))
+        project(hid, bd, part2)
+        for d in range(1, T):
+            piece(lax.rem(me + d, T)).start()
+    second = firsts[me].astype(F32) + part2[me].astype(F32)
+    for d in range(1, T):
+        peer = lax.rem(me + d, T)
+        piece_in(peer).wait_recv()
+        second = second + got2[peer].astype(F32)
     total = jnp.sum(second * second, axis=1, keepdims=True)
     conv[:, 0:dt] = second
     st2[...] = across_lanes(total, total)
@@ -328,7 +364,7 @@
         tp_send(1, st1, sg1.at[me], d).wait_send()
         tp_send(2, part1.at[peer], got1.at[d - 1], d).wait_send()
         tp_send(3, firsts.at[me], firsts.at[me], d).wait_send()
-        tp_send(4, part2.at[peer], got2.at[d - 1], d).wait_send()
+        piece(peer).wait_send()
         tp_send(5, st2, sg2.at[me], d).wait_send()
 
 
@@ -362,7 +398,7 @@
             pltpu.VMEM((T, count, dt), BF16),
             pltpu.VMEM((T, count, dt), BF16),
             pltpu.VMEM((T - 1, count, dt), BF16),
-            pltpu.VMEM((T - 1, count, dt), BF16),
+            pltpu.VMEM((T, count, dt), BF16),
             pltpu.VMEM((T, count, dt), BF16),
             pltpu.VMEM((count, ff), BF16),
             pltpu.VMEM((8, count), F32),

time: 193 us -> 168 us (0.87)
  Pallas kernels: 190 us -> 164 us
    pallas_call x1, Pallas kernels: 190 us -> 164 us  [body(): pl.pallas_call(functools.partial(kernel, R, F, T, split, length), out_sha...]
where the time goes in v2:
time: 168 us; the launch traced here: 167 us
  Pallas kernels  164 us (98%)
  local copies, waits for them, and re-layouts  3.59 us (2%)
    pallas_call x1, Pallas kernels, body(): pl.pallas_call(functools.partial(kernel, R, F, T, split, length), out_sha...  164 us

profile of v2, /device:TPU:0, one launch (start us, length us, event | category | flops | bytes accessed | tf_op | source)
XLA Modules:
  0.0 167.4 jit_solution(5839455191405500891)
XLA Ops:
  0.0 0.0 copy-start
  0.0 1.3 reshape.19.ng_ref
  1.3 0.0 copy-done
  1.3 0.6 reshape.21.mg_ref
  1.9 163.8 %block.1 = bf16[256,512]{1,0:T(8,128)(2,1)} custom-call(bf16[256,512]{1,0:T(8,128)(2,1)} %bitcast.5, f32[4,512]{1,0:T(4,128)} %reshape.19.ng_ref, f32[31,512]{1,0:T(8,128)} %cw_ref.1, f32[1,512]{1,0:T(1,128)} %bitcast.6, f32[4,512]{1,0:T(4,128)} %reshape.21.mg_ref, f32[1,512]{1,0:T(1,128)} %bitcast.7, bf16[512,512]{1,0:T(8,128)(2,1)} %wv_ref.1, ...), custom_call_target="tpu_custom_call" | custom-call | tf_op jit(solution)/shard_map/block/pallas_call | solution.py:387
  165.7 1.7 copy.14
Async XLA Ops:
  0.0 1.3 copy-start
